TPU v7x, 32 devices: a whole 2x2x4 slice. The times are simulated.
32 devices in a mesh: ep: 8 (over z, y), tp: 4 (over x, core).
Axes of the slice: x: 2, y: 2, z: 4, core: 2. Of those that a mesh axis runs over, the one named last changes fastest.
Arguments:
- q_latent: bfloat16 [4096, 1024], P(('ep', 'tp')), may hold values from -6 to 6
- kv_latent: bfloat16 [4096, 512], P(('ep', 'tp')), may hold values from -8 to 8
- rope_key: bfloat16 [4096, 64], P(('ep', 'tp')), may hold values from -2500 to 2500
- gain_query: float32 [1024], replicated, may hold values from 0.1 to 1.9
- gain_latent: float32 [512], replicated, may hold values from 0.1 to 1.9
- w_query: bfloat16 [1024, 3072], P(None, 'tp'), may hold values from -0.1875 to 0.1875
- w_key: bfloat16 [512, 2048], P(None, 'tp'), may hold values from -0.625 to 0.625
- w_value: bfloat16 [512, 2048], P(None, 'tp'), may hold values from -0.25 to 0.25
- w_out: bfloat16 [2048, 4096], P('tp'), may hold values from -0.25 to 0.25
- tokens_b: bfloat16 [4096, 4096], P(('ep', 'tp')), may hold values from -6 to 6
- gain_norm: float32 [4096], replicated, may hold values from 0.1 to 1.9
- routes: int32 [4096, 2], P(('ep', 'tp')), may hold values from 0 to 7, all different within a row; in each aligned block of 128 rows (0 to 127, 128 to 255, ...) at most 40 rows name the same one
- route_weights: float32 [4096, 2], P(('ep', 'tp')), may hold values from 0.2 to 1
- shared_gate: bfloat16 [4096, 1024], P(None, 'tp'), may hold values from -0.09375 to 0.09375
- shared_up: bfloat16 [4096, 1024], P(None, 'tp'), may hold values from -0.09375 to 0.09375
- shared_down: bfloat16 [1024, 4096], P('tp'), may hold values from -0.1875 to 0.1875
- expert_gate: bfloat16 [8, 4096, 1024], P('ep', None, 'tp'), may hold values from -0.09375 to 0.09375
- expert_up: bfloat16 [8, 4096, 1024], P('ep', None, 'tp'), may hold values from -0.09375 to 0.09375
- expert_down: bfloat16 [8, 1024, 4096], P('ep', 'tp'), may hold values from -0.1875 to 0.1875
Outputs:
- mixer_out: bfloat16 [4096, 4096], P(('ep', 'tp'))
- expert_mix: bfloat16 [4096, 4096], P(('ep', 'tp'))
Inputs may be any that keep to these rules, and one draw needn't show every extreme that they name: `routes`: in each aligned block of 128 rows no expert is named by more than 40 rows.
All inputs are finite; a program needn't handle non-finite values.
Results may differ from a plain program's by a relative error of at most 0.018.
The roundings to bfloat16 on the way count: a program that leaves them out, or rounds other values in their place, can miss the bound.
Values may be sent and summed in bfloat16 or wider, within the bound.
A program may use at most 192 MiB of HBM per device.

v0:
```python
import jax
import jax.numpy as jnp
from jax import lax
from jax.sharding import PartitionSpec as P

NOPE = 128
ROPE = 64
VDIM = 128
SEQS = 1


epsilon = 1e-06
rope_theta = 10000.0


def passed_along(value, axis, steps):
    count = lax.axis_size(axis)
    initial, last = (max(0, -steps), min(count, count - steps))
    return lax.ppermute(value, axis, [(source, source + steps) for source in range(initial, last)])


def rms_scale(values, gain_vec):
    floats = values.astype(jnp.float32)
    scaled = floats * lax.rsqrt(jnp.mean(floats * floats, axis=-1, keepdims=True) + epsilon)
    return (scaled * gain_vec).astype(jnp.bfloat16)


def rope_angles(positions, rope_width):
    frequency = rope_theta ** (-jnp.arange(0, rope_width, 2, dtype=jnp.float32) / rope_width)
    angles = positions.astype(jnp.float32)[:, None] * frequency[None, :]
    return (jnp.cos(angles), jnp.sin(angles))


def rotate_pairs(values, cos_tab, sin_tab):
    half_width = values.shape[-1] // 2
    first_half = values[..., :half_width]
    second_half = values[..., half_width:]
    return jnp.concatenate(
        [
            first_half * cos_tab - second_half * sin_tab,
            second_half * cos_tab + first_half * sin_tab,
        ],
        axis=-1,
    )


def block_scores(query_nope, query_rot, kv_block, pe_block, w_key, w_value, head_local):
    key_rows = kv_block.shape[0]
    key_proj = jnp.dot(kv_block, w_key, preferred_element_type=jnp.float32).astype(jnp.bfloat16)
    key_proj = key_proj.reshape(key_rows, head_local, -1)
    values = jnp.dot(kv_block, w_value, preferred_element_type=jnp.float32).astype(jnp.bfloat16)
    values = values.reshape(key_rows, head_local, -1)
    scores = jnp.einsum("qhd,khd->hqk", query_nope, key_proj, preferred_element_type=jnp.float32)
    scores = scores + jnp.einsum(
        "qhr,kr->hqk", query_rot, pe_block, preferred_element_type=jnp.float32
    )
    return (scores * (NOPE + ROPE) ** (-0.5), values)


def absorb(running, scores, values):
    top_old, sum_old, acc_old = running
    top_new = jnp.maximum(top_old, jnp.max(scores, axis=-1))
    factor = jnp.exp(top_old - top_new)
    exp_terms = jnp.exp(scores - top_new[:, :, None])
    sum_new = sum_old * factor + jnp.sum(exp_terms, axis=-1)
    update = jnp.einsum(
        "hqk,khd->qhd", exp_terms.astype(jnp.bfloat16), values, preferred_element_type=jnp.float32
    )
    return (top_new, sum_new, acc_old * factor.T[:, :, None] + update)


def slot_targets(route_ids, expert_total, capacity):
    pair_ids = route_ids.reshape(route_ids.shape[:-2] + (-1,))
    onehot = (pair_ids[..., None] == jnp.arange(expert_total, dtype=jnp.int32)).astype(jnp.int32)
    earlier = jnp.cumsum(onehot, axis=-2) - onehot
    return pair_ids * capacity + jnp.sum(earlier * onehot, axis=-1)


def dispatch_matrix(targets, tok_rows, top_k, slot_total):
    matches = targets[..., None, :] == jnp.arange(slot_total, dtype=jnp.int32)[:, None]
    matches = matches.reshape(matches.shape[:-1] + (tok_rows, top_k))
    return jnp.any(matches, axis=-1).astype(jnp.bfloat16)


def on_device(
    q_latent,
    kv_latent,
    rope_key,
    gain_query,
    gain_latent,
    w_query,
    w_key,
    w_value,
    w_out,
    tokens_b,
    gain_norm,
    routes,
    route_weights,
    shared_gate,
    shared_up,
    shared_down,
    expert_gate,
    expert_up,
    expert_down,
):
    tok_rows = q_latent.shape[0]
    tp_count = lax.axis_size("tp")
    ep_count = lax.axis_size("ep")
    group_rows = tok_rows * tp_count
    seq_span = ep_count // SEQS
    local_rank = lax.axis_index("ep") % seq_span
    head_local = w_value.shape[1] // VDIM
    q_normed = rms_scale(q_latent, gain_query)
    kv_normed = rms_scale(kv_latent, gain_latent)
    group_q, group_kv, group_pe = (
        lax.all_gather(q_normed, "tp", axis=0, tiled=True),
        lax.all_gather(kv_normed, "tp", axis=0, tiled=True),
        lax.all_gather(rope_key, "tp", axis=0, tiled=True),
    )
    positions = local_rank * group_rows + jnp.arange(group_rows, dtype=jnp.int32)
    cos_tab, sin_tab = rope_angles(positions, ROPE)
    query_full = jnp.dot(group_q, w_query, preferred_element_type=jnp.float32)
    query_full = query_full.reshape(group_rows, head_local, NOPE + ROPE)
    query_rot = rotate_pairs(
        query_full[:, :, NOPE:], cos_tab[:, None, :], sin_tab[:, None, :]
    ).astype(jnp.bfloat16)
    query_nope = query_full[:, :, :NOPE].astype(jnp.bfloat16)
    rot_keys = rotate_pairs(group_pe.astype(jnp.float32), cos_tab, sin_tab).astype(jnp.bfloat16)

    def attend(running, kv_block, pe_block):
        scores, values = block_scores(
            query_nope, query_rot, kv_block, pe_block, w_key, w_value, head_local
        )
        return absorb(running, scores, values)

    own_scores, own_values = block_scores(
        query_nope, query_rot, group_kv, rot_keys, w_key, w_value, head_local
    )
    row_ids = jnp.arange(group_rows, dtype=jnp.int32)
    causal = row_ids[:, None] >= row_ids[None, :]
    own_scores = jnp.where(causal[None], own_scores, -jnp.inf)
    start_state = (
        jnp.full((head_local, group_rows), -jnp.inf, jnp.float32),
        jnp.zeros((head_local, group_rows), jnp.float32),
        jnp.zeros((group_rows, head_local, VDIM), jnp.float32),
    )
    running = absorb(start_state, own_scores, own_values)

    def chain_turn(turn_num, loop_state):
        held_state, kv_block, pe_block = loop_state
        kv_block, pe_block = passed_along((kv_block, pe_block), "ep", 1)
        held_state = lax.cond(
            local_rank >= turn_num,
            lambda: attend(held_state, kv_block, pe_block),
            lambda: held_state,
        )
        return (held_state, kv_block, pe_block)

    running = lax.fori_loop(1, seq_span, chain_turn, (running, group_kv, rot_keys))[0]
    sum_all = running[1]
    acc_all = running[2]
    heads_out = (
        (acc_all / sum_all.T[:, :, None])
        .astype(jnp.bfloat16)
        .reshape(group_rows, head_local * VDIM)
    )
    mixer_out = lax.psum_scatter(
        jnp.dot(heads_out, w_out, preferred_element_type=jnp.float32).astype(jnp.bfloat16),
        "tp",
        scatter_dimension=0,
        tiled=True,
    )
    top_k = routes.shape[1]
    model_width = tokens_b.shape[1]
    exp_dev = expert_gate.shape[0]
    expert_total = exp_dev * ep_count
    capacity = 5 * tok_rows * top_k // (4 * expert_total)
    slot_total = expert_total * capacity
    normed_b = rms_scale(tokens_b, gain_norm)
    own_targets = slot_targets(routes, expert_total, capacity)
    mapping = dispatch_matrix(own_targets, tok_rows, top_k, slot_total)
    outgoing = jnp.dot(mapping, normed_b, preferred_element_type=jnp.float32).astype(jnp.bfloat16)
    outgoing = outgoing.reshape(ep_count, exp_dev * capacity, model_width)
    incoming = lax.all_to_all(outgoing, "ep", split_axis=0, concat_axis=0, tiled=True)
    shared_rows, arrived = (
        lax.all_gather(normed_b, "tp", axis=0, tiled=True),
        lax.all_gather(incoming, "tp", axis=0, tiled=True),
    )
    routed = arrived.reshape(tp_count, ep_count, exp_dev, capacity, model_width)
    gate_shared = jnp.dot(shared_rows, shared_gate, preferred_element_type=jnp.float32)
    up_shared = jnp.dot(shared_rows, shared_up, preferred_element_type=jnp.float32)
    shared_hidden = (jax.nn.silu(gate_shared) * up_shared).astype(jnp.bfloat16)
    shared_hidden = shared_hidden.reshape(tp_count, tok_rows, -1)
    routed_gate = jnp.einsum(
        "qsjcm,jmf->qsjcf", routed, expert_gate, preferred_element_type=jnp.float32
    )
    routed_up = jnp.einsum(
        "qsjcm,jmf->qsjcf", routed, expert_up, preferred_element_type=jnp.float32
    )
    routed_hidden = (jax.nn.silu(routed_gate) * routed_up).astype(jnp.bfloat16)
    block_rows = tok_rows + ep_count * exp_dev * capacity
    group_count = block_rows * lax.axis_size("tp") // block_rows
    shared_out = jnp.einsum(
        "qrf,fm->qrm", shared_hidden, shared_down, preferred_element_type=jnp.float32
    )
    routed_out = jnp.einsum(
        "qsjcf,jfm->qsjcm", routed_hidden, expert_down, preferred_element_type=jnp.float32
    )
    routed_out = routed_out.reshape(group_count, -1, model_width)
    summed = lax.psum_scatter(
        jnp.concatenate([shared_out, routed_out], axis=1)
        .reshape(block_rows * lax.axis_size("tp"), model_width)
        .astype(jnp.bfloat16),
        "tp",
        scatter_dimension=0,
        tiled=True,
    )
    shared_result = summed[:tok_rows]
    routed_back = summed[tok_rows:].reshape(ep_count, exp_dev * capacity, model_width)
    returned = lax.all_to_all(routed_back, "ep", split_axis=0, concat_axis=0, tiled=True).reshape(
        slot_total, model_width
    )
    picked = jnp.take(returned, own_targets, axis=0).reshape(tok_rows, top_k, model_width)
    routed_sum = jnp.sum(route_weights[:, :, None] * picked.astype(jnp.float32), axis=1)
    expert_mix = (shared_result.astype(jnp.float32) + routed_sum).astype(jnp.bfloat16)
    return (mixer_out, expert_mix)


def solution(mesh):
    return jax.shard_map(
        on_device,
        mesh=mesh,
        in_specs=(
            P(("ep", "tp"), None),
            P(("ep", "tp"), None),
            P(("ep", "tp"), None),
            P(),
            P(),
            P(None, "tp"),
            P(None, "tp"),
            P(None, "tp"),
            P("tp", None),
            P(("ep", "tp"), None),
            P(),
            P(("ep", "tp"), None),
            P(("ep", "tp"), None),
            P(None, "tp"),
            P(None, "tp"),
            P("tp", None),
            P("ep", None, "tp"),
            P("ep", None, "tp"),
            P("ep", "tp", None),
        ),
        out_specs=(P(("ep", "tp"), None), P(("ep", "tp"), None)),
        check_vma=False,
    )
```

profile of v0, /device:TPU:13, one launch (start us, length us, event | category | flops | bytes accessed | tf_op | source)
XLA Modules:
  0.0 457.9 jit_solution(9782188747694806250)
XLA Ops:
  7.2 1.7 fusion.18
  8.9 2.5 fusion.20
  13.7 2.1 convolution_convert_fusion.5
  15.8 62.1 %all_to_all.10 = bf16[8,40,4096]{2,1,0:T(8,128)(2,1)} all-to-all(bf16[8,40,4096]{2,1,0:T(8,128)(2,1)S(1)} %bitcast.155), channel_id=1, replica_groups=mesh['ep'=8,'tp'=4] {'ep'}, dimensions={0} | all-to-all | bytes 5242880 | tf_op jit(solution)/shard_map/all_to_all | solution.py:184
  79.3 4.3 fusion.77
  85.6 3.4 convolution_convert_fusion.3
  88.9 61.9 %all-gather.8.cloned.1.call-done = bf16[32,40,4096]{2,1,0:T(8,128)(2,1)} async-done(((bf16[8,40,4096]{2,1,0:T(8,128)(2,1)}), bf16[32,40,4096]{2,1,0:T(8,128)(2,1)}) %all-gather.8.cloned.1.call-update) | async-done | bytes 10485776 | tf_op jit(solution)/shard_map/all_gather | solution.py:187
  150.8 6.3 %fusion.30 = f32[4,8,1,40,256]{4,3,1,0,2:T(8,128)S(1)} fusion(bf16[4,8,40,4096]{3,2,1,0:T(8,128)(2,1)} %bitcast.168, bf16[1,4096,256]{2,1,0:T(8,128)(2,1)} %param.39), kind=kOutput, calls=%fused_computation.43 | convolution fusion | flops 2684354560 | bytes 13893632 | tf_op jit(solution)/shard_map/qsjcm,jmf->qsjcf/dot_general | solution.py:194
  157.2 16.8 %convolution_convert_fusion.2 = bf16[4,8,40,4096]{3,2,1,0:T(8,128)(2,1)} fusion(bf16[1,256,4096]{2,1,0:T(8,128)(2,1)S(1)} %copy-done, bf16[4,8,40,4096]{3,2,1,0:T(8,128)(2,1)} %bitcast.169, bf16[1,4096,256]{2,1,0:T(8,128)(2,1)} %param.40, f32[4,8,1,40,256]{4,3,1,0,2:T(8,128)S(1)} %fusion.30), kind=kOutput, calls=%fused_computation.17 | convolution fusion | flops 5375918080 | bytes 26476544 | tf_op jit(solution)/shard_map/qsjcf,jfm->qsjcm/dot_general | solution.py:206
  173.9 12.7 %pad_maximum_fusion = bf16[4,448,4096]{2,1,0:T(8,128)(2,1)} fusion(bf16[4,320,4096]{2,1,0:T(8,128)(2,1)} %bitcast.156, bf16[4,128,4096]{2,1,0:T(8,128)(2,1)} %convolution_convert_fusion.3), kind=kLoop, calls=%fused_computation.16 | loop fusion | flops 29360128 | bytes 29360128 | tf_op jit(solution)/shard_map/concatenate | solution.py:211
  187.4 5.3 %all_gather.17 = bf16[512,64]{0,1:T(8,128)(2,1)S(1)} all-gather(bf16[128,64]{0,1:T(8,128)(2,1)S(1)} %copy-done.10), channel_id=1, replica_groups=mesh['ep'=8,'tp'=4] {'tp'}, dimensions={0}, use_global_device_ids=true | all-gather | bytes 81920 | tf_op jit(solution)/shard_map/all_gather | solution.py:118
  194.2 7.5 %all_gather.16 = bf16[512,512]{1,0:T(8,128)(2,1)S(1)} all-gather(bf16[128,512]{1,0:T(8,128)(2,1)S(1)} %fusion.61), channel_id=1, replica_groups=mesh['ep'=8,'tp'=4] {'tp'}, dimensions={0}, use_global_device_ids=true | all-gather | bytes 655360 | tf_op jit(solution)/shard_map/all_gather | solution.py:117
  204.3 3.5 fusion.76
  208.7 1.3 copy.68
  210.1 1.8 fusion.73
  215.1 129.8 %while.21 = (s32[]{:T(128)}, f32[4,512]{1,0:T(4,128)S(1)}, f32[4,512]{1,0:T(4,128)S(1)}, f32[512,4,128]{0,2,1:T(8,128)S(1)}, bf16[512,512]{1,0:T(8,128)(2,1)}, /...) while((s32[]{:T(128)}, f32[4,512]{1,0:T(4,128)S(1)}, ...), condition=%wide.region_9.10_spmd, body=%wide.region_4.9_spmd.sunk | while | flops 1216354304 | bytes 31785300 | solution.py:159
  215.1 3.1 collective-permute-start
  218.2 3.1 collective-permute-start.1
  221.3 11.0 %collective-permute-done.1 = bf16[512,64]{0,1:T(8,128)(2,1)S(1)} collective-permute-done((bf16[512,64]{0,1:T(8,128)(2,1)S(1)}, bf16[512,64]{0,1:T(8,128)(2,1)S(1)}, u32[]{:S(2)}, u32[]{:S(2)}) %collective-permute-start.1) | collective-permute-done | bytes 65568 | tf_op jit(solution)/shard_map/while/body/eval_jaxpr/ppermute | solution.py:19
  232.3 4.2 conditional.2
  237.4 3.9 collective-permute-start
  241.3 2.2 collective-permute-start.1
  243.5 10.3 %collective-permute-done.1 = bf16[512,64]{0,1:T(8,128)(2,1)S(1)} collective-permute-done((bf16[512,64]{0,1:T(8,128)(2,1)S(1)}, bf16[512,64]{0,1:T(8,128)(2,1)S(1)}, u32[]{:S(2)}, u32[]{:S(2)}) %collective-permute-start.1) | collective-permute-done | bytes 65568 | tf_op jit(solution)/shard_map/while/body/eval_jaxpr/ppermute | solution.py:19
  253.8 4.2 conditional.2
  258.9 4.6 %collective-permute-start = (bf16[512,512]{1,0:T(8,128)(2,1)}, bf16[512,512]{1,0:T(8,128)(2,1)S(1)}, u32[]{:S(2)}, u32[]{:S(2)}) collective-permute-start(bf16[512,512]{1,0:T(8,128)(2,1)} %get-tuple-element.377), channel_id=1, source_target_pairs={{0,4},{4,8},{8,12},{12,16},{16,20},{20,24},{24,28},{1,5},{5,9},{9,... | collective-permute-start | bytes 1572872 | tf_op jit(solution)/shard_map/while/body/eval_jaxpr/ppermute | solution.py:19
  263.5 1.9 collective-permute-start.1
  265.4 9.6 %collective-permute-done.1 = bf16[512,64]{0,1:T(8,128)(2,1)S(1)} collective-permute-done((bf16[512,64]{0,1:T(8,128)(2,1)S(1)}, bf16[512,64]{0,1:T(8,128)(2,1)S(1)}, u32[]{:S(2)}, u32[]{:S(2)}) %collective-permute-start.1) | collective-permute-done | bytes 65568 | tf_op jit(solution)/shard_map/while/body/eval_jaxpr/ppermute | solution.py:19
  275.1 4.2 conditional.2
  280.1 4.7 %collective-permute-start = (bf16[512,512]{1,0:T(8,128)(2,1)}, bf16[512,512]{1,0:T(8,128)(2,1)S(1)}, u32[]{:S(2)}, u32[]{:S(2)}) collective-permute-start(bf16[512,512]{1,0:T(8,128)(2,1)} %get-tuple-element.377), channel_id=1, source_target_pairs={{0,4},{4,8},{8,12},{12,16},{16,20},{20,24},{24,28},{1,5},{5,9},{9,... | collective-permute-start | bytes 1572872 | tf_op jit(solution)/shard_map/while/body/eval_jaxpr/ppermute | solution.py:19
  284.8 1.9 collective-permute-start.1
  286.8 8.5 %collective-permute-done.1 = bf16[512,64]{0,1:T(8,128)(2,1)S(1)} collective-permute-done((bf16[512,64]{0,1:T(8,128)(2,1)S(1)}, bf16[512,64]{0,1:T(8,128)(2,1)S(1)}, u32[]{:S(2)}, u32[]{:S(2)}) %collective-permute-start.1) | collective-permute-done | bytes 65568 | tf_op jit(solution)/shard_map/while/body/eval_jaxpr/ppermute | solution.py:19
  296.1 9.2 %collective-permute-start = (bf16[512,512]{1,0:T(8,128)(2,1)}, bf16[512,512]{1,0:T(8,128)(2,1)S(1)}, u32[]{:S(2)}, u32[]{:S(2)}) collective-permute-start(bf16[512,512]{1,0:T(8,128)(2,1)} %get-tuple-element.377), channel_id=1, source_target_pairs={{0,4},{4,8},{8,12},{12,16},{16,20},{20,24},{24,28},{1,5},{5,9},{9,... | collective-permute-start | bytes 1572872 | tf_op jit(solution)/shard_map/while/body/eval_jaxpr/ppermute | solution.py:19
  305.3 1.9 collective-permute-start.1
  307.3 7.7 %collective-permute-done.1 = bf16[512,64]{0,1:T(8,128)(2,1)S(1)} collective-permute-done((bf16[512,64]{0,1:T(8,128)(2,1)S(1)}, bf16[512,64]{0,1:T(8,128)(2,1)S(1)}, u32[]{:S(2)}, u32[]{:S(2)}) %collective-permute-start.1) | collective-permute-done | bytes 65568 | tf_op jit(solution)/shard_map/while/body/eval_jaxpr/ppermute | solution.py:19
  315.8 5.0 %collective-permute-start = (bf16[512,512]{1,0:T(8,128)(2,1)}, bf16[512,512]{1,0:T(8,128)(2,1)S(1)}, u32[]{:S(2)}, u32[]{:S(2)}) collective-permute-start(bf16[512,512]{1,0:T(8,128)(2,1)} %get-tuple-element.377), channel_id=1, source_target_pairs={{0,4},{4,8},{8,12},{12,16},{16,20},{20,24},{24,28},{1,5},{5,9},{9,... | collective-permute-start | bytes 1572872 | tf_op jit(solution)/shard_map/while/body/eval_jaxpr/ppermute | solution.py:19
  320.8 5.5 %collective-permute-start.1 = (bf16[512,64]{0,1:T(8,128)(2,1)S(1)}, bf16[512,64]{0,1:T(8,128)(2,1)S(1)}, u32[]{:S(2)}, u32[]{:S(2)}) collective-permute-start(bf16[512,64]{0,1:T(8,128)(2,1)S(1)} %get-tuple-element.378), channel_id=1, source_target_pairs={{0,4},{4,8},{8,12},{12,16},{16,20},{20,24},{24,28},{1,5},{5,9},{9,... | collective-permute-start | bytes 196616 | tf_op jit(solution)/shard_map/while/body/eval_jaxpr/ppermute | solution.py:19
  326.3 3.2 collective-permute-done.1
  330.4 5.6 %collective-permute-start = (bf16[512,512]{1,0:T(8,128)(2,1)}, bf16[512,512]{1,0:T(8,128)(2,1)S(1)}, u32[]{:S(2)}, u32[]{:S(2)}) collective-permute-start(bf16[512,512]{1,0:T(8,128)(2,1)} %get-tuple-element.377), channel_id=1, source_target_pairs={{0,4},{4,8},{8,12},{12,16},{16,20},{20,24},{24,28},{1,5},{5,9},{9,... | collective-permute-start | bytes 1572872 | tf_op jit(solution)/shard_map/while/body/eval_jaxpr/ppermute | solution.py:19
  336.0 4.8 %collective-permute-start.1 = (bf16[512,64]{0,1:T(8,128)(2,1)S(1)}, bf16[512,64]{0,1:T(8,128)(2,1)S(1)}, u32[]{:S(2)}, u32[]{:S(2)}) collective-permute-start(bf16[512,64]{0,1:T(8,128)(2,1)S(1)} %get-tuple-element.378), channel_id=1, source_target_pairs={{0,4},{4,8},{8,12},{12,16},{16,20},{20,24},{24,28},{1,5},{5,9},{9,... | collective-permute-start | bytes 196616 | tf_op jit(solution)/shard_map/while/body/eval_jaxpr/ppermute | solution.py:19
  340.8 3.2 collective-permute-done.1
  345.0 6.5 %convolution_convert_fusion.4 = bf16[512,4096]{1,0:T(8,128)(2,1)} fusion(bf16[512,512]{0,1:T(8,128)(2,1)S(1)} %bitcast.161, bf16[512,4096]{1,0:T(8,128)(2,1)} %param.31), kind=kOutput, calls=%fused_computation.19 | convolution fusion | flops 2149580800 | bytes 8912896 | tf_op jit(solution)/shard_map/dot_general | solution.py:168
  351.6 3.6 slice.49
  355.1 17.9 %all-to-all-start.1 = ((bf16[8,40,4096]{2,1,0:T(8,128)(2,1)}), bf16[8,40,4096]{2,1,0:T(8,128)(2,1)S(1)}, u32[]{:S(2)}, u32[]{:S(2)}) async-start(bf16[8,40,4096]{2,1,0:T(8,128)(2,1)} %bitcast.157), calls=%async_computation.3 | async-start | bytes 5242880 | tf_op jit(solution)/shard_map/all_to_all | solution.py:220
  373.6 56.3 %all-to-all-done.1 = bf16[8,40,4096]{2,1,0:T(8,128)(2,1)S(1)} async-done(((bf16[8,40,4096]{2,1,0:T(8,128)(2,1)}), bf16[8,40,4096]{2,1,0:T(8,128)(2,1)S(1)}, u32[]{:S(2)}, u32[]{:S(2)}) %all-to-all-start.1) | async-done | bytes 2621472 | tf_op jit(solution)/shard_map/all_to_all | solution.py:220
  430.0 3.2 gather_fusion
  433.2 4.5 gather.7
  437.7 10.8 %multiply_reduce_fusion = f32[128,4096]{1,0:T(8,128)S(1)} fusion(bf16[128,2,4096]{2,1,0:T(2,128)(2,1)} %gather.7, pred[128,2]{1,0:T(8,128)(4,1)S(1)} %copy.73, f32[128,2]{1,0:T(8,128)S(1)} %copy.72), kind=kLoop, calls=%fused_computation.24 | loop fusion | flops 3670016 | bytes 4195584 | tf_op jit(solution)/shard_map/reduce_sum | solution.py:224
  448.5 2.4 add_convert_fusion
  (152 shorter events, 33.2 us)
Async XLA Ops:
  7.2 150.0 %copy-start = (bf16[1,256,4096]{2,1,0:T(8,128)(2,1)S(1)}, bf16[1,256,4096]{2,1,0:T(8,128)(2,1)}, u32[]{:S(2)}) copy-start(bf16[1,256,4096]{2,1,0:T(8,128)(2,1)} %param.41) | copy-start | bytes 6291460
  7.2 4.3 copy-start.11
  7.2 72.1 %all-gather.6.cloned.1.call-start = ((), (), s32[]{:S(2)}) async-start(), calls=%async_computation.6 | async-start | bytes 5242880 | tf_op jit(solution)/shard_map/all_gather | solution.py:186
  11.5 139.3 %all-gather.8.cloned.1.call-start = ((), (), s32[]{:S(2)}) async-start(), calls=%async_computation.7 | async-start | bytes 13107200 | tf_op jit(solution)/shard_map/all_gather | solution.py:187
  12.9 2.9 copy-start.13
  15.8 62.2 %copy-start.8 = (bf16[128,1024]{1,0:T(8,128)(2,1)S(1)}, bf16[128,1024]{1,0:T(8,128)(2,1)}, u32[]{:S(2)}) copy-start(bf16[128,1024]{1,0:T(8,128)(2,1)} %param.23) | copy-start | bytes 786436
  15.8 62.3 %copy-start.15 = (f32[1024]{0:T(1024)S(1)}, f32[1024]{0:T(1024)}, u32[]{:S(2)}) copy-start(f32[1024]{0:T(1024)} %param.26) | copy-start | bytes 12292
  77.9 126.3 %all-gather.4.cloned.1.call-start = ((), (), s32[]{:S(2)}) async-start(), calls=%async_computation.4 | async-start | bytes 1310720 | tf_op jit(solution)/shard_map/all_gather | solution.py:116
  79.0 272.5 %reduce-scatter.5.cloned.1.call-start = ((), (), s32[]{:S(2)}) async-start(), calls=%async_computation.8 | async-start | bytes 18350080 | tf_op jit(solution)/shard_map/reduce_scatter | solution.py:210
  79.3 4.3 copy-start.19
  79.3 4.7 %copy-start.20 = (bf16[4096,256]{1,0:T(8,128)(2,1)S(1)}, bf16[4096,256]{1,0:T(8,128)(2,1)}, u32[]{:S(2)}) copy-start(bf16[4096,256]{1,0:T(8,128)(2,1)} %param.37) | copy-start | bytes 6291460
  84.0 1.6 copy-start.5
  186.7 0.7 copy-start.10
  186.7 7.2 %copy-start.9 = (bf16[128,512]{1,0:T(8,128)(2,1)S(1)}, bf16[128,512]{1,0:T(8,128)(2,1)}, u32[]{:S(2)}) copy-start(bf16[128,512]{1,0:T(8,128)(2,1)} %param.24) | copy-start | bytes 393220
  186.7 7.4 %copy-start.16 = (f32[512]{0:T(512)S(1)}, f32[512]{0:T(512)}, u32[]{:S(2)}) copy-start(f32[512]{0:T(512)} %param.27) | copy-start | bytes 6148
  186.7 15.0 %copy-start.2 = (bf16[512,512]{1,0:T(8,128)(2,1)S(1)}, bf16[512,512]{1,0:T(8,128)(2,1)}, u32[]{:S(2)}) copy-start(bf16[512,512]{1,0:T(8,128)(2,1)} %param.29) | copy-start | bytes 1572868
  186.7 16.3 %copy-start.3 = (bf16[512,512]{1,0:T(8,128)(2,1)S(1)}, bf16[512,512]{1,0:T(8,128)(2,1)}, u32[]{:S(2)}) copy-start(bf16[512,512]{1,0:T(8,128)(2,1)} %param.30) | copy-start | bytes 1572868
  186.8 264.2 %reduce-scatter.3.cloned.1.call-start = ((), (), s32[]{:S(2)}) async-start(), calls=%async_computation.5 | async-start | bytes 5242880 | tf_op jit(solution)/shard_map/reduce_scatter | solution.py:167
  201.7 1.3 copy-start.4
  210.0 2.0 copy-start.7
  213.2 1.0 copy-start.6
  215.1 17.2 %collective-permute-start = (bf16[512,512]{1,0:T(8,128)(2,1)}, bf16[512,512]{1,0:T(8,128)(2,1)S(1)}, u32[]{:S(2)}, u32[]{:S(2)}) collective-permute-start(bf16[512,512]{1,0:T(8,128)(2,1)} %get-tuple-element.377), channel_id=1, source_target_pairs={{0,4},{4,8},{8,12},{12,16},{16,20},{20,24},{24,28},{1,5},{5,9},{9,... | collective-permute-start | bytes 1572872 | tf_op jit(solution)/shard_map/while/body/eval_jaxpr/ppermute | solution.py:19
  218.2 14.1 %collective-permute-start.1 = (bf16[512,64]{0,1:T(8,128)(2,1)S(1)}, bf16[512,64]{0,1:T(8,128)(2,1)S(1)}, u32[]{:S(2)}, u32[]{:S(2)}) collective-permute-start(bf16[512,64]{0,1:T(8,128)(2,1)S(1)} %get-tuple-element.378), channel_id=1, source_target_pairs={{0,4},{4,8},{8,12},{12,16},{16,20},{20,24},{24,28},{1,5},{5,9},{9,... | collective-permute-start | bytes 196616 | tf_op jit(solution)/shard_map/while/body/eval_jaxpr/ppermute | solution.py:19
  237.4 16.5 %collective-permute-start = (bf16[512,512]{1,0:T(8,128)(2,1)}, bf16[512,512]{1,0:T(8,128)(2,1)S(1)}, u32[]{:S(2)}, u32[]{:S(2)}) collective-permute-start(bf16[512,512]{1,0:T(8,128)(2,1)} %get-tuple-element.377), channel_id=1, source_target_pairs={{0,4},{4,8},{8,12},{12,16},{16,20},{20,24},{24,28},{1,5},{5,9},{9,... | collective-permute-start | bytes 1572872 | tf_op jit(solution)/shard_map/while/body/eval_jaxpr/ppermute | solution.py:19
  241.3 12.5 %collective-permute-start.1 = (bf16[512,64]{0,1:T(8,128)(2,1)S(1)}, bf16[512,64]{0,1:T(8,128)(2,1)S(1)}, u32[]{:S(2)}, u32[]{:S(2)}) collective-permute-start(bf16[512,64]{0,1:T(8,128)(2,1)S(1)} %get-tuple-element.378), channel_id=1, source_target_pairs={{0,4},{4,8},{8,12},{12,16},{16,20},{20,24},{24,28},{1,5},{5,9},{9,... | collective-permute-start | bytes 196616 | tf_op jit(solution)/shard_map/while/body/eval_jaxpr/ppermute | solution.py:19
  258.9 16.2 %collective-permute-start = (bf16[512,512]{1,0:T(8,128)(2,1)}, bf16[512,512]{1,0:T(8,128)(2,1)S(1)}, u32[]{:S(2)}, u32[]{:S(2)}) collective-permute-start(bf16[512,512]{1,0:T(8,128)(2,1)} %get-tuple-element.377), channel_id=1, source_target_pairs={{0,4},{4,8},{8,12},{12,16},{16,20},{20,24},{24,28},{1,5},{5,9},{9,... | collective-permute-start | bytes 1572872 | tf_op jit(solution)/shard_map/while/body/eval_jaxpr/ppermute | solution.py:19
  263.5 11.6 %collective-permute-start.1 = (bf16[512,64]{0,1:T(8,128)(2,1)S(1)}, bf16[512,64]{0,1:T(8,128)(2,1)S(1)}, u32[]{:S(2)}, u32[]{:S(2)}) collective-permute-start(bf16[512,64]{0,1:T(8,128)(2,1)S(1)} %get-tuple-element.378), channel_id=1, source_target_pairs={{0,4},{4,8},{8,12},{12,16},{16,20},{20,24},{24,28},{1,5},{5,9},{9,... | collective-permute-start | bytes 196616 | tf_op jit(solution)/shard_map/while/body/eval_jaxpr/ppermute | solution.py:19
  280.1 15.2 %collective-permute-start = (bf16[512,512]{1,0:T(8,128)(2,1)}, bf16[512,512]{1,0:T(8,128)(2,1)S(1)}, u32[]{:S(2)}, u32[]{:S(2)}) collective-permute-start(bf16[512,512]{1,0:T(8,128)(2,1)} %get-tuple-element.377), channel_id=1, source_target_pairs={{0,4},{4,8},{8,12},{12,16},{16,20},{20,24},{24,28},{1,5},{5,9},{9,... | collective-permute-start | bytes 1572872 | tf_op jit(solution)/shard_map/while/body/eval_jaxpr/ppermute | solution.py:19
  284.8 10.5 %collective-permute-start.1 = (bf16[512,64]{0,1:T(8,128)(2,1)S(1)}, bf16[512,64]{0,1:T(8,128)(2,1)S(1)}, u32[]{:S(2)}, u32[]{:S(2)}) collective-permute-start(bf16[512,64]{0,1:T(8,128)(2,1)S(1)} %get-tuple-element.378), channel_id=1, source_target_pairs={{0,4},{4,8},{8,12},{12,16},{16,20},{20,24},{24,28},{1,5},{5,9},{9,... | collective-permute-start | bytes 196616 | tf_op jit(solution)/shard_map/while/body/eval_jaxpr/ppermute | solution.py:19
  296.1 18.8 %collective-permute-start = (bf16[512,512]{1,0:T(8,128)(2,1)}, bf16[512,512]{1,0:T(8,128)(2,1)S(1)}, u32[]{:S(2)}, u32[]{:S(2)}) collective-permute-start(bf16[512,512]{1,0:T(8,128)(2,1)} %get-tuple-element.377), channel_id=1, source_target_pairs={{0,4},{4,8},{8,12},{12,16},{16,20},{20,24},{24,28},{1,5},{5,9},{9,... | collective-permute-start | bytes 1572872 | tf_op jit(solution)/shard_map/while/body/eval_jaxpr/ppermute | solution.py:19
  305.3 9.6 %collective-permute-start.1 = (bf16[512,64]{0,1:T(8,128)(2,1)S(1)}, bf16[512,64]{0,1:T(8,128)(2,1)S(1)}, u32[]{:S(2)}, u32[]{:S(2)}) collective-permute-start(bf16[512,64]{0,1:T(8,128)(2,1)S(1)} %get-tuple-element.378), channel_id=1, source_target_pairs={{0,4},{4,8},{8,12},{12,16},{16,20},{20,24},{24,28},{1,5},{5,9},{9,... | collective-permute-start | bytes 196616 | tf_op jit(solution)/shard_map/while/body/eval_jaxpr/ppermute | solution.py:19
  315.8 13.8 %collective-permute-start = (bf16[512,512]{1,0:T(8,128)(2,1)}, bf16[512,512]{1,0:T(8,128)(2,1)S(1)}, u32[]{:S(2)}, u32[]{:S(2)}) collective-permute-start(bf16[512,512]{1,0:T(8,128)(2,1)} %get-tuple-element.377), channel_id=1, source_target_pairs={{0,4},{4,8},{8,12},{12,16},{16,20},{20,24},{24,28},{1,5},{5,9},{9,... | collective-permute-start | bytes 1572872 | tf_op jit(solution)/shard_map/while/body/eval_jaxpr/ppermute | solution.py:19
  320.8 8.7 %collective-permute-start.1 = (bf16[512,64]{0,1:T(8,128)(2,1)S(1)}, bf16[512,64]{0,1:T(8,128)(2,1)S(1)}, u32[]{:S(2)}, u32[]{:S(2)}) collective-permute-start(bf16[512,64]{0,1:T(8,128)(2,1)S(1)} %get-tuple-element.378), channel_id=1, source_target_pairs={{0,4},{4,8},{8,12},{12,16},{16,20},{20,24},{24,28},{1,5},{5,9},{9,... | collective-permute-start | bytes 196616 | tf_op jit(solution)/shard_map/while/body/eval_jaxpr/ppermute | solution.py:19
  330.4 13.6 %collective-permute-start = (bf16[512,512]{1,0:T(8,128)(2,1)}, bf16[512,512]{1,0:T(8,128)(2,1)S(1)}, u32[]{:S(2)}, u32[]{:S(2)}) collective-permute-start(bf16[512,512]{1,0:T(8,128)(2,1)} %get-tuple-element.377), channel_id=1, source_target_pairs={{0,4},{4,8},{8,12},{12,16},{16,20},{20,24},{24,28},{1,5},{5,9},{9,... | collective-permute-start | bytes 1572872 | tf_op jit(solution)/shard_map/while/body/eval_jaxpr/ppermute | solution.py:19
  336.0 8.0 %collective-permute-start.1 = (bf16[512,64]{0,1:T(8,128)(2,1)S(1)}, bf16[512,64]{0,1:T(8,128)(2,1)S(1)}, u32[]{:S(2)}, u32[]{:S(2)}) collective-permute-start(bf16[512,64]{0,1:T(8,128)(2,1)S(1)} %get-tuple-element.378), channel_id=1, source_target_pairs={{0,4},{4,8},{8,12},{12,16},{16,20},{20,24},{24,28},{1,5},{5,9},{9,... | collective-permute-start | bytes 196616 | tf_op jit(solution)/shard_map/while/body/eval_jaxpr/ppermute | solution.py:19
  355.1 17.9 %copy-start.12 = (s32[128,2]{0,1:T(2,128)S(1)}, s32[128,2]{0,1:T(2,128)}, u32[]{:S(2)}) copy-start(s32[128,2]{0,1:T(2,128)} %param.34) | copy-start | bytes 3076
  355.1 18.2 %copy-start.17 = (pred[128,2]{0,1:T(4,128)(4,1)S(1)}, pred[128,2]{0,1:T(4,128)(4,1)}, u32[]{:S(2)}) copy-start(pred[128,2]{0,1:T(4,128)(4,1)} %get-tuple-element.266) | copy-start | bytes 772
  355.1 18.4 %copy-start.18 = (f32[128,2]{0,1:T(2,128)S(1)}, f32[128,2]{0,1:T(2,128)}, u32[]{:S(2)}) copy-start(f32[128,2]{0,1:T(2,128)} %param.35) | copy-start | bytes 3076
  355.1 18.5 %copy-start.14 = (s32[256]{0:T(256)S(1)}, s32[256]{0:T(256)}, u32[]{:S(2)}) copy-start(s32[256]{0:T(256)} %copy-done.13) | copy-start | bytes 3076
  355.1 74.8 %all-to-all-start.1 = ((bf16[8,40,4096]{2,1,0:T(8,128)(2,1)}), bf16[8,40,4096]{2,1,0:T(8,128)(2,1)S(1)}, u32[]{:S(2)}, u32[]{:S(2)}) async-start(bf16[8,40,4096]{2,1,0:T(8,128)(2,1)} %bitcast.157), calls=%async_computation.3 | async-start | bytes 5242880 | tf_op jit(solution)/shard_map/all_to_all | solution.py:220
  433.2 17.8 %copy-start.1 = (bf16[1,256,4096]{2,1,0:T(8,128)(2,1)S(1)}, bf16[1,256,4096]{2,1,0:T(8,128)(2,1)}, u32[]{:S(2)}) copy-start(bf16[1,256,4096]{2,1,0:T(8,128)(2,1)} %param.41) | copy-start | bytes 6291460
Sparse Core Ops, SparseCore 0:
  11.6 35.9 all-gather.5
  78.1 72.7 all-gather.7
  152.4 16.6 all-gather.3
  186.9 113.3 reduce-scatter.4
  351.7 61.2 reduce-scatter.2
where the time goes:
time: 466 us; the launch traced here: 458 us
  waiting for transfers between devices  172 us (37%)
  starting transfers between devices  75.8 us (16%)
  blocking collectives  75 us (16%)
  matrix products  61.1 us (13%)
  other arithmetic  36.5 us (8%)
  local copies, waits for them, and re-layouts  22.5 us (5%)
  between operations  14.7 us (3%)
    all_to_all x1, blocking collectives, on_device(): lax.all_to_all(outgoing, 'ep', split_axis=0, concat_axis=0, tiled=True)  62.1 us
    all_gather x1, waiting for transfers between devices, on_device(): lax.all_gather(incoming, 'tp', axis=0, tiled=True)  61.9 us
    ppermute x14, starting transfers between devices, passed_along(): lax.ppermute(value, axis, [(source, source + steps) for source in range(i...  57.5 us
    all_to_all x1, waiting for transfers between devices, on_device(): lax.all_to_all(routed_back, 'ep', split_axis=0, concat_axis=0, tiled=True)  56.3 us
    ppermute x14, waiting for transfers between devices, passed_along(): lax.ppermute(value, axis, [(source, source + steps) for source in range(i...  53.6 us
    all_to_all x1, starting transfers between devices, on_device(): lax.all_to_all(routed_back, 'ep', split_axis=0, concat_axis=0, tiled=True)  17.9 us
    dot_general x1, matrix products, on_device(): jnp.einsum('qsjcf,jfm->qsjcm', routed_hidden, expert_down, preferred_elem...  16.8 us
    concatenate x1, other arithmetic, on_device(): jnp.concatenate([shared_out, routed_out], axis=1)  12.7 us
  transfers between devices with their start and end apart: 20, of which 9 were waited for; matrix products, arithmetic and copies ran while one was open for 25% of the time, Pallas kernels for 0%

commit v1 on v0

v1 whole, which is shorter than its diff:
```python
import functools

import jax
import jax.numpy as jnp
from jax import lax
from jax.experimental import pallas as pl
from jax.experimental.pallas import tpu as pltpu
from jax.sharding import PartitionSpec as P

NOPE = 128
ROPE = 64
VDIM = 128
SEQS = 1


epsilon = 1e-06
rope_theta = 10000.0


def exchange_kernel(axis, count, src_ref, dst_ref, send_sem, recv_sem, local_sem):
    me = lax.axis_index(axis)
    barrier = pltpu.get_barrier_semaphore()
    for step in range(1, count):
        pl.semaphore_signal(
            barrier,
            inc=1,
            device_id={axis: lax.rem(me + step, count)},
            device_id_type=pl.DeviceIdType.MESH,
        )
    pl.semaphore_wait(barrier, count - 1)
    copies = []
    for step in range(1, count):
        target = lax.rem(me + step, count)
        copy = pltpu.make_async_remote_copy(
            src_ref=src_ref.at[target],
            dst_ref=dst_ref.at[me],
            send_sem=send_sem.at[step],
            recv_sem=recv_sem.at[step],
            device_id={axis: target},
            device_id_type=pl.DeviceIdType.MESH,
        )
        copy.start()
        copies.append(copy)
    own = pltpu.make_async_copy(src_ref.at[me], dst_ref.at[me], local_sem)
    own.start()
    own.wait()
    for copy in copies:
        copy.wait()


def exchange(blocks, axis, collective_id):
    count = blocks.shape[0]
    return pl.pallas_call(
        functools.partial(exchange_kernel, axis, count),
        out_shape=jax.ShapeDtypeStruct(blocks.shape, blocks.dtype),
        in_specs=[pl.BlockSpec(memory_space=pltpu.VMEM)],
        out_specs=pl.BlockSpec(memory_space=pltpu.VMEM),
        scratch_shapes=[
            pltpu.SemaphoreType.DMA((count,)),
            pltpu.SemaphoreType.DMA((count,)),
            pltpu.SemaphoreType.DMA,
        ],
        compiler_params=pltpu.CompilerParams(
            collective_id=collective_id, has_side_effects=True, vmem_limit_bytes=16 * 2**20
        ),
        cost_estimate=pl.CostEstimate(
            flops=0, bytes_accessed=40 * blocks.size * 2, transcendentals=0
        ),
    )(blocks)


def rms_scale(values, gain_vec):
    floats = values.astype(jnp.float32)
    scaled = floats * lax.rsqrt(jnp.mean(floats * floats, axis=-1, keepdims=True) + epsilon)
    return (scaled * gain_vec).astype(jnp.bfloat16)


def rope_angles(positions, rope_width):
    frequency = rope_theta ** (-jnp.arange(0, rope_width, 2, dtype=jnp.float32) / rope_width)
    angles = positions.astype(jnp.float32)[:, None] * frequency[None, :]
    return (jnp.cos(angles), jnp.sin(angles))


def rotate_pairs(values, cos_tab, sin_tab):
    half_width = values.shape[-1] // 2
    first_half = values[..., :half_width]
    second_half = values[..., half_width:]
    return jnp.concatenate(
        [
            first_half * cos_tab - second_half * sin_tab,
            second_half * cos_tab + first_half * sin_tab,
        ],
        axis=-1,
    )


def block_scores(query_nope, query_rot, kv_block, pe_block, w_key, w_value, head_local):
    key_rows = kv_block.shape[0]
    key_proj = jnp.dot(kv_block, w_key, preferred_element_type=jnp.float32).astype(jnp.bfloat16)
    key_proj = key_proj.reshape(key_rows, head_local, -1)
    values = jnp.dot(kv_block, w_value, preferred_element_type=jnp.float32).astype(jnp.bfloat16)
    values = values.reshape(key_rows, head_local, -1)
    scores = jnp.einsum("qhd,khd->hqk", query_nope, key_proj, preferred_element_type=jnp.float32)
    scores = scores + jnp.einsum(
        "qhr,kr->hqk", query_rot, pe_block, preferred_element_type=jnp.float32
    )
    return (scores * (NOPE + ROPE) ** (-0.5), values)


def absorb(running, scores, values):
    top_old, sum_old, acc_old = running
    top_new = jnp.maximum(top_old, jnp.max(scores, axis=-1))
    factor = jnp.exp(top_old - top_new)
    exp_terms = jnp.exp(scores - top_new[:, :, None])
    sum_new = sum_old * factor + jnp.sum(exp_terms, axis=-1)
    update = jnp.einsum(
        "hqk,khd->qhd", exp_terms.astype(jnp.bfloat16), values, preferred_element_type=jnp.float32
    )
    return (top_new, sum_new, acc_old * factor.T[:, :, None] + update)


def slot_targets(route_ids, expert_total, capacity):
    pair_ids = route_ids.reshape(route_ids.shape[:-2] + (-1,))
    onehot = (pair_ids[..., None] == jnp.arange(expert_total, dtype=jnp.int32)).astype(jnp.int32)
    earlier = jnp.cumsum(onehot, axis=-2) - onehot
    return pair_ids * capacity + jnp.sum(earlier * onehot, axis=-1)


def dispatch_matrix(targets, tok_rows, top_k, slot_total):
    matches = targets[..., None, :] == jnp.arange(slot_total, dtype=jnp.int32)[:, None]
    matches = matches.reshape(matches.shape[:-1] + (tok_rows, top_k))
    return jnp.any(matches, axis=-1).astype(jnp.bfloat16)


def on_device(
    q_latent,
    kv_latent,
    rope_key,
    gain_query,
    gain_latent,
    w_query,
    w_key,
    w_value,
    w_out,
    tokens_b,
    gain_norm,
    routes,
    route_weights,
    shared_gate,
    shared_up,
    shared_down,
    expert_gate,
    expert_up,
    expert_down,
):
    tok_rows = q_latent.shape[0]
    tp_count = lax.axis_size("tp")
    ep_count = lax.axis_size("ep")
    group_rows = tok_rows * tp_count
    seq_span = ep_count // SEQS
    local_rank = lax.axis_index("ep") % seq_span
    head_local = w_value.shape[1] // VDIM
    q_normed = rms_scale(q_latent, gain_query)
    kv_normed = rms_scale(kv_latent, gain_latent)
    frequency_cos, frequency_sin = rope_angles(
        local_rank * group_rows
        + lax.axis_index("tp") * tok_rows
        + jnp.arange(tok_rows, dtype=jnp.int32),
        ROPE,
    )
    rot_own = rotate_pairs(rope_key.astype(jnp.float32), frequency_cos, frequency_sin)
    latent = jnp.concatenate([kv_normed, rot_own.astype(jnp.bfloat16)], axis=1)

    top_k = routes.shape[1]
    model_width = tokens_b.shape[1]
    exp_dev = expert_gate.shape[0]
    expert_total = exp_dev * ep_count
    capacity = 5 * tok_rows * top_k // (4 * expert_total)
    slot_total = expert_total * capacity
    normed_b = rms_scale(tokens_b, gain_norm)
    own_targets = slot_targets(routes, expert_total, capacity)
    mapping = dispatch_matrix(own_targets, tok_rows, top_k, slot_total)
    outgoing = jnp.dot(mapping, normed_b, preferred_element_type=jnp.float32).astype(jnp.bfloat16)
    outgoing = outgoing.reshape(ep_count, exp_dev * capacity, model_width)
    incoming = exchange(outgoing, "ep", 1)

    shared_rows = lax.all_gather(normed_b, "tp", axis=0, tiled=True)
    group_q = lax.all_gather(q_normed, "tp", axis=0, tiled=True)
    all_latent = lax.all_gather(latent, ("ep", "tp"), axis=0, tiled=True)
    arrived = lax.all_gather(incoming, "tp", axis=0, tiled=True)

    positions = local_rank * group_rows + jnp.arange(group_rows, dtype=jnp.int32)
    cos_tab, sin_tab = rope_angles(positions, ROPE)
    query_full = jnp.dot(group_q, w_query, preferred_element_type=jnp.float32)
    query_full = query_full.reshape(group_rows, head_local, NOPE + ROPE)
    query_rot = rotate_pairs(
        query_full[:, :, NOPE:], cos_tab[:, None, :], sin_tab[:, None, :]
    ).astype(jnp.bfloat16)
    query_nope = query_full[:, :, :NOPE].astype(jnp.bfloat16)

    gate_shared = jnp.dot(shared_rows, shared_gate, preferred_element_type=jnp.float32)
    up_shared = jnp.dot(shared_rows, shared_up, preferred_element_type=jnp.float32)
    shared_hidden = (jax.nn.silu(gate_shared) * up_shared).astype(jnp.bfloat16)
    shared_part = jnp.dot(shared_hidden, shared_down, preferred_element_type=jnp.float32).astype(
        jnp.bfloat16
    )
    shared_parts = exchange(shared_part.reshape(tp_count, tok_rows, model_width), "tp", 3)
    all_latent, shared_parts = lax.optimization_barrier((all_latent, shared_parts))
    shared_result = jnp.sum(shared_parts.astype(jnp.float32), axis=0).astype(jnp.bfloat16)

    first_rank = lax.axis_index("ep") - local_rank
    row_ids = jnp.arange(group_rows, dtype=jnp.int32)

    def attend_block(turn, running):
        block = lax.dynamic_slice_in_dim(
            all_latent, (first_rank + turn) * group_rows, group_rows, axis=0
        )
        scores, values = block_scores(
            query_nope,
            query_rot,
            block[:, : kv_latent.shape[1]],
            block[:, kv_latent.shape[1] :],
            w_key,
            w_value,
            head_local,
        )
        allowed = positions[:, None] >= (turn * group_rows + row_ids)[None, :]
        scores = jnp.where(allowed[None], scores, -jnp.inf)
        return absorb(running, scores, values)

    start_state = (
        jnp.full((head_local, group_rows), -jnp.inf, jnp.float32),
        jnp.zeros((head_local, group_rows), jnp.float32),
        jnp.zeros((group_rows, head_local, VDIM), jnp.float32),
    )
    running = lax.fori_loop(0, local_rank + 1, attend_block, start_state)
    sum_all = running[1]
    acc_all = running[2]
    heads_out = (
        (acc_all / sum_all.T[:, :, None])
        .astype(jnp.bfloat16)
        .reshape(group_rows, head_local * VDIM)
    )
    mixer_part = jnp.dot(heads_out, w_out, preferred_element_type=jnp.float32).astype(
        jnp.bfloat16
    )

    arrived, mixer_part = lax.optimization_barrier((arrived, mixer_part))

    routed = arrived.reshape(tp_count * ep_count, exp_dev, capacity, model_width)
    routed_gate = jnp.einsum(
        "sjcm,jmf->sjcf", routed, expert_gate, preferred_element_type=jnp.float32
    )
    routed_up = jnp.einsum("sjcm,jmf->sjcf", routed, expert_up, preferred_element_type=jnp.float32)
    routed_hidden = (jax.nn.silu(routed_gate) * routed_up).astype(jnp.bfloat16)
    routed_part = jnp.einsum(
        "sjcf,jfm->sjcm", routed_hidden, expert_down, preferred_element_type=jnp.float32
    ).astype(jnp.bfloat16)
    routed_part = routed_part.reshape(tp_count * slot_total, model_width)
    routed_back = lax.psum_scatter(routed_part, "tp", scatter_dimension=0, tiled=True)
    mixer_out = lax.psum_scatter(mixer_part, "tp", scatter_dimension=0, tiled=True)
    returned = exchange(routed_back.reshape(ep_count, exp_dev * capacity, model_width), "ep", 2)
    returned = returned.reshape(slot_total, model_width)
    hits = own_targets.reshape(tok_rows, top_k)[:, :, None] == jnp.arange(
        slot_total, dtype=jnp.int32
    )
    combine = jnp.sum(jnp.where(hits, route_weights[:, :, None], 0.0), axis=1)
    routed_sum = jnp.zeros((tok_rows, model_width), jnp.float32)
    for _ in range(3):
        term = lax.reduce_precision(combine, 8, 7)
        routed_sum = routed_sum + jnp.dot(
            term.astype(jnp.bfloat16), returned, preferred_element_type=jnp.float32
        )
        combine = combine - term
    expert_mix = (shared_result.astype(jnp.float32) + routed_sum).astype(jnp.bfloat16)
    return (mixer_out, expert_mix)


def solution(mesh):
    return jax.shard_map(
        on_device,
        mesh=mesh,
        in_specs=(
            P(("ep", "tp"), None),
            P(("ep", "tp"), None),
            P(("ep", "tp"), None),
            P(),
            P(),
            P(None, "tp"),
            P(None, "tp"),
            P(None, "tp"),
            P("tp", None),
            P(("ep", "tp"), None),
            P(),
            P(("ep", "tp"), None),
            P(("ep", "tp"), None),
            P(None, "tp"),
            P(None, "tp"),
            P("tp", None),
            P("ep", None, "tp"),
            P("ep", None, "tp"),
            P("ep", "tp", None),
        ),
        out_specs=(P(("ep", "tp"), None), P(("ep", "tp"), None)),
        check_vma=False,
    )
```

time: 466 us -> 423 us (0.908); the launches traced: 458 us -> 422 us
  Pallas kernels: 0 us -> 186 us
  starting transfers between devices: 75.8 us -> 0.25 us
  blocking collectives: 75 us -> 0 us
  waiting for transfers between devices: 172 us -> 115 us
  other arithmetic: 36.5 us -> 16.4 us
  matrix products: 61.1 us -> 79 us
  local copies, waits for them, and re-layouts: 22.5 us -> 10.8 us
    pallas_call x0 -> x3, Pallas kernels: none -> 186 us  [exchange(): pl.pallas_call(functools.partial(exchange_kernel, axis, count), out_shape...]
    reduce_scatter x2, waiting for transfers between devices: 0.02 us -> 101 us  [the longest x1 101 us: on_device(): lax.psum_scatter(routed_part, 'tp', scatter_dimension=0, tiled=True)]
    all_to_all x1 -> x0, blocking collectives: 62.1 us -> none  [on_device(): lax.all_to_all(outgoing, 'ep', split_axis=0, concat_axis=0, tiled=True)]
    ppermute x14 -> x0, starting transfers between devices: 57.5 us -> none  [passed_along(): lax.ppermute(value, axis, [(source, source + steps) for source in range(i...]
    all_to_all x1 -> x0, waiting for transfers between devices: 56.3 us -> none  [on_device(): lax.all_to_all(routed_back, 'ep', split_axis=0, concat_axis=0, tiled=True)]
    ppermute x14 -> x0, waiting for transfers between devices: 53.6 us -> none  [passed_along(): lax.ppermute(value, axis, [(source, source + steps) for source in range(i...]
    all_gather x3 -> x4, waiting for transfers between devices: 61.9 us -> 13.7 us  [the longest x1 13.6 us: on_device(): arrived = lax.all_gather(incoming, 'tp', axis=0, tiled=True)]
    all_to_all x1 -> x0, starting transfers between devices: 17.9 us -> none  [on_device(): lax.all_to_all(routed_back, 'ep', split_axis=0, concat_axis=0, tiled=True)]
  transfers between devices with their start and end apart: 20 -> 6, of which waited for: 9 -> 2; matrix products, arithmetic and copies ran while one was open for 25% -> 17% of each run, Pallas kernels for 0% -> 44%
where the time goes in v1:
time: 423 us; the launch traced here: 422 us
  Pallas kernels  186 us (44%)
  waiting for transfers between devices  115 us (27%)
  matrix products  79 us (19%)
  other arithmetic  16.4 us (4%)
  between operations  14.5 us (3%)
  local copies, waits for them, and re-layouts  10.8 us (3%)
    pallas_call x3, Pallas kernels, exchange(): pl.pallas_call(functools.partial(exchange_kernel, axis, count), out_shape...  186 us
    reduce_scatter x1, waiting for transfers between devices, on_device(): lax.psum_scatter(routed_part, 'tp', scatter_dimension=0, tiled=True)  101 us
    dot_general x1, matrix products, on_device(): jnp.einsum('sjcf,jfm->sjcm', routed_hidden, expert_down, preferred_elemen...  16.6 us
    all_gather x1, waiting for transfers between devices, on_device(): arrived = lax.all_gather(incoming, 'tp', axis=0, tiled=True)  13.6 us
    dot_general x1, matrix products, on_device(): jnp.dot(shared_hidden, shared_down, preferred_element_type=jnp.float32)  9.92 us
    unnamed x29, local copies, waits for them, and re-layouts  9.86 us
  transfers between devices with their start and end apart: 6, of which 2 were waited for; matrix products, arithmetic and copies ran while one was open for 17% of the time, Pallas kernels for 44%

profile of v1, /device:TPU:13, one launch (start us, length us, event | category | flops | bytes accessed | tf_op | source)
XLA Modules:
  0.0 422.0 jit_solution(15538991564990390681)
XLA Ops:
  7.3 1.2 fusion.51
  8.5 1.8 fusion.53
  10.4 1.5 fusion.24
  11.9 2.0 fusion.26
  17.0 0.8 convolution_convert_fusion.5
  17.9 61.0 %shard_map.194 = bf16[8,40,4096]{2,1,0:T(8,128)(2,1)S(1)} custom-call(bf16[8,40,4096]{2,1,0:T(8,128)(2,1)S(1)} %bitcast.138), custom_call_target="tpu_custom_call" | custom-call | bytes 104857600 | tf_op jit(solution)/shard_map/pallas_call | solution.py:53
  78.9 1.5 copy-done.2
  80.8 2.8 fusion.84
  83.6 1.1 copy-done.8
  84.8 1.0 copy.68
  85.8 1.1 subtract_convert_fusion
  87.0 4.1 fusion.83
  91.1 9.9 %convolution_convert_fusion.3 = bf16[512,4096]{1,0:T(8,128)(2,1)} fusion(bf16[256,4096]{1,0:T(8,128)(2,1)} %param.36, bf16[512,4096]{1,0:T(8,128)(2,1)} %all-gather.9.cloned.1.call-done, bf16[4096,256]{1,0:T(8,128)(2,1)} %param.35, f32[512,256]{1,0:T(8,128)S(1)} %fusion.83), kind=kOutput, calls=%fused_computation.26 | convolution fusion | flops 2150367232 | bytes 13107200 | tf_op jit(solution)/shard_map/dot_general | solution.py:204
  101.0 2.2 copy-done.3
  103.2 63.7 %shard_map.195 = bf16[4,128,4096]{2,1,0:T(8,128)(2,1)S(1)} custom-call(bf16[4,128,4096]{2,1,0:T(8,128)(2,1)S(1)} %bitcast.139), custom_call_target="tpu_custom_call" | custom-call | bytes 167772160 | tf_op jit(solution)/shard_map/pallas_call | solution.py:53
  166.9 2.0 copy-done.1
  169.0 32.8 %while.15 = (s32[]{:T(128)}, f32[4,512]{1,0:T(4,128)S(1)}, f32[4,512]{1,0:T(4,128)S(1)}, f32[512,4,128]{0,2,1:T(8,128)S(1)}, s32[]{:T(128)}, /*index=5*/s32[]{:T...) while((s32[]{:T(128)}, f32[4,512]{1,0:T(4,128)S(1)}, ...), condition=%wide.region_10.11_spmd.clone, body=%wide.region_7.10_spmd.clone.sunk | while | flops 1217666048 | bytes 30875948 | solution.py:236
  169.5 1.7 convolution_convert_fusion.9
  171.2 1.8 convolution_convert_fusion.8
  173.0 0.8 fusion.130
  173.8 2.0 fusion.131
  176.3 1.0 fusion.134
  177.7 1.7 convolution_convert_fusion.9
  179.4 1.7 convolution_convert_fusion.8
  181.1 0.8 fusion.130
  181.9 2.0 fusion.131
  184.5 1.0 fusion.134
  185.8 1.7 convolution_convert_fusion.9
  187.5 1.7 convolution_convert_fusion.8
  189.2 0.8 fusion.130
  190.0 2.0 fusion.131
  192.6 1.0 fusion.134
  193.9 1.7 convolution_convert_fusion.9
  195.6 1.7 convolution_convert_fusion.8
  197.3 0.8 fusion.130
  198.1 2.0 fusion.131
  200.7 1.0 fusion.134
  201.9 6.5 %convolution_convert_fusion.4 = bf16[512,4096]{1,0:T(8,128)(2,1)} fusion(bf16[512,512]{0,1:T(8,128)(2,1)S(1)} %bitcast.144, bf16[512,4096]{1,0:T(8,128)(2,1)} %param.29), kind=kOutput, calls=%fused_computation.27 | convolution fusion | flops 2149580800 | bytes 8912896 | tf_op jit(solution)/shard_map/dot_general | solution.py:244
  208.5 13.6 %all-gather.5.cloned.1.call-done = bf16[32,40,4096]{2,1,0:T(8,128)(2,1)} async-done(((bf16[8,40,4096]{2,1,0:T(8,128)(2,1)}), bf16[32,40,4096]{2,1,0:T(8,128)(2,1)}) %all-gather.5.cloned.1.call-update) | async-done | bytes 10485776 | tf_op jit(solution)/shard_map/all_gather | solution.py:190
  222.1 6.3 %fusion.32 = f32[32,1,40,256]{3,2,0,1:T(8,128)S(1)} fusion(bf16[32,40,4096]{2,1,0:T(8,128)(2,1)} %all-gather.5.cloned.1.call-done, bf16[1,4096,256]{2,1,0:T(8,128)(2,1)} %param.37), kind=kOutput, calls=%fused_computation.43 | convolution fusion | flops 2684354560 | bytes 13893632 | tf_op jit(solution)/shard_map/sjcm,jmf->sjcf/dot_general | solution.py:251
  228.4 16.6 %convolution_convert_fusion.2 = bf16[32,40,4096]{2,1,0:T(8,128)(2,1)} fusion(bf16[1,256,4096]{2,1,0:T(8,128)(2,1)S(1)} %copy-done, bf16[32,40,4096]{2,1,0:T(8,128)(2,1)} %all-gather.5.cloned.1.call-done, bf16[1,4096,256]{2,1,0:T(8,128)(2,1)} %param.38, f32[32,1,40,256]{3,2,0,1:T(8,128)S(1)} %fusion.32), kind=kOutput, calls=%fused_computation.25 | convolution fusion | flops 5375918080 | bytes 26476544 | tf_op jit(solution)/shard_map/sjcf,jfm->sjcm/dot_general | solution.py:256
  245.7 3.1 reduce_sum.73
  248.8 100.5 %reduce-scatter.5.cloned.1.call-done = bf16[320,4096]{1,0:T(8,128)(2,1)} async-done(((bf16[1280,4096]{1,0:T(8,128)(2,1)}), bf16[320,4096]{1,0:T(8,128)(2,1)}) %reduce-scatter.5.cloned.1.call-update) | async-done | bytes 2621456 | tf_op jit(solution)/shard_map/reduce_scatter | solution.py:260
  349.3 1.7 copy-done.4
  351.0 60.8 %shard_map.196 = bf16[8,40,4096]{2,1,0:T(8,128)(2,1)S(1)} custom-call(bf16[8,40,4096]{2,1,0:T(8,128)(2,1)S(1)} %bitcast.140), custom_call_target="tpu_custom_call" | custom-call | bytes 104857600 | tf_op jit(solution)/shard_map/pallas_call | solution.py:53
  411.9 0.8 fusion.67
  412.6 0.8 convolution_add_fusion.1
  413.4 1.8 fusion.23
  (102 shorter events, 7.8 us)
Async XLA Ops:
  7.2 221.2 %copy-start = (bf16[1,256,4096]{2,1,0:T(8,128)(2,1)S(1)}, bf16[1,256,4096]{2,1,0:T(8,128)(2,1)}, u32[]{:S(2)}) copy-start(bf16[1,256,4096]{2,1,0:T(8,128)(2,1)} %param.39) | copy-start | bytes 6291460
  7.2 4.7 %copy-start.7 = (bf16[128,4096]{1,0:T(8,128)(2,1)S(1)}, bf16[128,4096]{1,0:T(8,128)(2,1)}, u32[]{:S(2)}) copy-start(bf16[128,4096]{1,0:T(8,128)(2,1)} %param.30) | copy-start | bytes 3145732
  7.2 6.8 %copy-start.10 = (bf16[128,64]{0,1:T(8,128)(2,1)S(1)}, bf16[128,64]{0,1:T(8,128)(2,1)}, u32[]{:S(2)}) copy-start(bf16[128,64]{0,1:T(8,128)(2,1)} %param.23) | copy-start | bytes 49156
  7.2 6.8 %copy-start.9 = (bf16[128,512]{1,0:T(8,128)(2,1)S(1)}, bf16[128,512]{1,0:T(8,128)(2,1)}, u32[]{:S(2)}) copy-start(bf16[128,512]{1,0:T(8,128)(2,1)} %param.22) | copy-start | bytes 393220
  7.2 73.6 %all-gather.11.cloned.1.call-start = ((), (), s32[]{:S(2)}) async-start(), calls=%async_computation.5 | async-start | bytes 1310720 | tf_op jit(solution)/shard_map/all_gather | solution.py:188
  10.3 4.2 copy-start.12
  10.3 5.1 %copy-start.11 = (s32[128,2]{0,1:T(2,128)S(1)}, s32[128,2]{0,1:T(2,128)}, u32[]{:S(2)}) copy-start(s32[128,2]{0,1:T(2,128)} %param.32) | copy-start | bytes 3076
  10.3 76.6 %all-gather.9.cloned.1.call-start = ((), (), s32[]{:S(2)}) async-start(), calls=%async_computation.4 | async-start | bytes 5242880 | tf_op jit(solution)/shard_map/all_gather | solution.py:187
  13.9 3.1 copy-start.6
  14.0 154.9 %all-gather.7.cloned.1.call-start = ((), (), s32[]{:S(2)}) async-start(), calls=%async_computation.3 | async-start | bytes 4866048 | tf_op jit(solution)/shard_map/all_gather | solution.py:189
  15.3 206.8 %all-gather.5.cloned.1.call-start = ((), (), s32[]{:S(2)}) async-start(), calls=%async_computation.2 | async-start | bytes 13107200 | tf_op jit(solution)/shard_map/all_gather | solution.py:190
  78.9 1.5 copy-start.2
  80.4 268.9 %reduce-scatter.5.cloned.1.call-start = ((), (), s32[]{:S(2)}) async-start(), calls=%async_computation.7 | async-start | bytes 13107200 | tf_op jit(solution)/shard_map/reduce_scatter | solution.py:260
  83.6 1.1 copy-start.8
  101.0 2.2 copy-start.3
  166.9 2.0 copy-start.1
  169.2 3.7 copy-start.5
  177.5 3.6 copy-start.5
  185.6 3.6 copy-start.5
  193.7 3.6 copy-start.5
  245.0 0.7 copy-start.13
  245.0 170.2 %reduce-scatter.3.cloned.1.call-start = ((), (), s32[]{:S(2)}) async-start(), calls=%async_computation.6 | async-start | bytes 5242880 | tf_op jit(solution)/shard_map/reduce_scatter | solution.py:261
  349.3 1.7 copy-start.4
Sparse Core Ops, SparseCore 0:
  10.4 18.1 all-gather.10
  30.8 34.4 all-gather.8
  68.2 79.9 all-gather.6
  149.6 72.4 all-gather.4
  245.1 104.1 reduce-scatter.4
  352.2 44.5 reduce-scatter.2
